TPU v7x, 32 devices: a whole 2x2x4 slice. The times are simulated.
32 devices in a mesh: grp: 2 (over y), fs: 4 (over z), tp: 4 (over x, core).
Axes of the slice: x: 2, y: 2, z: 4, core: 2. Of those that a mesh axis runs over, the one named last changes fastest.
Arguments:
- tokens: bfloat16 [4096, 2048], P(('grp', 'fs', 'tp')), parts along dimension 0, may hold values from -6 to 6
- route_ids: int32 [4096, 8], P(('grp', 'fs', 'tp')), parts along dimension 0, may hold values from 0 to 15, all different within a row; in each aligned block of 128 rows (0 to 127, 128 to 255, ...) at most 96 rows name the same one
- route_scores: float32 [4096, 8], P(('grp', 'fs', 'tp')), parts along dimension 0, may hold values from 0.05 to 1
- norm_gain: float32 [2048], P('fs'), may hold values from 0.1 to 1.9
- expert_gate: float32 [16, 2048, 256], P(None, 'fs', 'tp'), may hold values from -0.125 to 0.125
- expert_up: float32 [16, 2048, 256], P(None, 'fs', 'tp'), may hold values from -0.125 to 0.125
- expert_down: float32 [16, 256, 2048], P(None, 'fs', 'tp'), may hold values from -0.375 to 0.375
- shared_gate: float32 [2048, 256], P('fs', 'tp'), may hold values from -0.125 to 0.125
- shared_up: float32 [2048, 256], P('fs', 'tp'), may hold values from -0.125 to 0.125
- shared_down: float32 [256, 2048], P('fs', 'tp'), may hold values from -0.375 to 0.375
Outputs:
- mixed: bfloat16 [4096, 2048], P(('grp', 'fs', 'tp')), parts along dimension 0
- sampler_gate: bfloat16 [32, 2048, 256], P(('grp', 'fs', 'tp')), parts along dimension 0
- sampler_up: bfloat16 [32, 2048, 256], P(('grp', 'fs', 'tp')), parts along dimension 0
- sampler_down: bfloat16 [32, 256, 2048], P(('grp', 'fs', 'tp')), parts along dimension 0
- sampler_shared_gate: bfloat16 [4096, 256], P(('grp', 'fs')), parts along dimension 0
- sampler_shared_up: bfloat16 [4096, 256], P(('grp', 'fs')), parts along dimension 0
- sampler_shared_down: bfloat16 [512, 2048], P(('grp', 'fs')), parts along dimension 0
There are 2 independent parts, one for each index of `grp`. A program takes and returns all parts, laid end to end along the dimension named above; an argument that names none is the same for every part. Nothing has to cross between parts.
Inputs may be any that keep to these rules, and one draw needn't show every extreme that they name: `route_ids`: each row names 8 different experts. Among the 128 rows of one device no expert is named more than 96 times, a bound that some block reaches.
All inputs are finite; a program needn't handle non-finite values.
Results may differ from a plain program's by a relative error of at most 0.0084.
Values may be sent and summed in bfloat16 or wider, within the bound.
A program may use at most 128 MiB of HBM per device.

v0:
```python
import jax
import jax.numpy as jnp
from jax import lax
from jax.sharding import PartitionSpec as P

EPSILON = 1e-06
route_scale = 2.5


def expert_rows(row_block, w_gate, w_up, w_down):
    gate_rows = jnp.dot(row_block, w_gate, preferred_element_type=jnp.float32)
    up_rows = jnp.dot(row_block, w_up, preferred_element_type=jnp.float32)
    hidden = (jax.nn.silu(gate_rows) * up_rows).astype(jnp.bfloat16)
    return jnp.dot(hidden, w_down, preferred_element_type=jnp.float32).astype(jnp.bfloat16)


def relayout(arrived, fs_count, tp_count):
    tile_rows = arrived.shape[2]
    tile_cols = arrived.shape[3]
    grid = arrived.reshape(fs_count, tp_count, tile_rows, tile_cols)
    grid = jnp.transpose(grid, (0, 2, 1, 3))
    return grid.reshape(1, fs_count * tile_rows, tp_count * tile_cols)


def on_device(
    tokens,
    route_ids,
    route_scores,
    norm_gain,
    expert_gate,
    expert_up,
    expert_down,
    shared_gate,
    shared_up,
    shared_down,
):
    fs_count = lax.axis_size("fs")
    tp_count = lax.axis_size("tp")
    experts = fs_count * tp_count
    gain_col = norm_gain[:, None]
    piece_gate = (gain_col[None] * expert_gate).astype(jnp.bfloat16)
    piece_up = (gain_col[None] * expert_up).astype(jnp.bfloat16)
    piece_down = expert_down.astype(jnp.bfloat16)
    moved = (
        lax.all_to_all(piece_gate[:, None], ("fs", "tp"), split_axis=0, concat_axis=1, tiled=True),
        lax.all_to_all(piece_up[:, None], ("fs", "tp"), split_axis=0, concat_axis=1, tiled=True),
        lax.all_to_all(piece_down[:, None], ("fs", "tp"), split_axis=0, concat_axis=1, tiled=True),
    )
    served_gate = relayout(moved[0], fs_count, tp_count)
    served_up = relayout(moved[1], fs_count, tp_count)
    served_down = relayout(moved[2], fs_count, tp_count)
    tile_gate = (gain_col * shared_gate).astype(jnp.bfloat16)
    tile_up = (gain_col * shared_up).astype(jnp.bfloat16)
    tile_down = shared_down.astype(jnp.bfloat16)
    held_gate, held_up, held_down = (
        lax.all_gather(tile_gate, "tp", axis=1, tiled=True),
        lax.all_gather(tile_up, "tp", axis=1, tiled=True),
        lax.all_gather(tile_down, "tp", axis=1, tiled=True),
    )
    rows_dev = tokens.shape[0]
    width = tokens.shape[1]
    picks = route_ids.shape[1]
    capacity = 3 * rows_dev * picks // (2 * experts)
    widened = tokens.astype(jnp.float32)
    normed = (
        widened * lax.rsqrt(jnp.mean(widened * widened, axis=1, keepdims=True) + EPSILON)
    ).astype(jnp.bfloat16)
    weights = route_scale * route_scores / jnp.sum(route_scores, axis=1, keepdims=True)
    flat_ids = route_ids.reshape(-1)
    onehot = (flat_ids[:, None] == jnp.arange(experts, dtype=jnp.int32)[None, :]).astype(jnp.int32)
    earlier = jnp.cumsum(onehot, axis=0) - onehot
    ranks = jnp.sum(earlier * onehot, axis=1)
    target = flat_ids * capacity + ranks
    outbox = (
        jnp.zeros((experts * capacity, width), jnp.bfloat16)
        .at[target]
        .set(jnp.repeat(normed, picks, axis=0))
    )
    arrived = lax.all_to_all(
        outbox.reshape(experts, capacity, width),
        ("fs", "tp"),
        split_axis=0,
        concat_axis=0,
        tiled=True,
    )
    finished = expert_rows(
        arrived.reshape(-1, width), served_gate[0], served_up[0], served_down[0]
    ).reshape(arrived.shape)
    returned = lax.all_to_all(finished, ("fs", "tp"), split_axis=0, concat_axis=0, tiled=True)
    results = returned.reshape(experts * capacity, width)[target]
    routed = jnp.sum(
        results.reshape(rows_dev, picks, width).astype(jnp.float32) * weights[:, :, None], axis=1
    )
    columns = normed
    gate_part = jnp.dot(
        columns,
        lax.all_gather(held_gate, "fs", axis=0, tiled=True),
        preferred_element_type=jnp.float32,
    )
    up_part = jnp.dot(
        columns,
        lax.all_gather(held_up, "fs", axis=0, tiled=True),
        preferred_element_type=jnp.float32,
    )
    shared_hidden = (jax.nn.silu(gate_part) * up_part).astype(jnp.bfloat16)
    columns = shared_hidden
    shared_term = jnp.dot(
        columns,
        lax.all_gather(held_down, "fs", axis=0, tiled=True),
        preferred_element_type=jnp.float32,
    )
    mixed = (routed + shared_term).astype(jnp.bfloat16)
    return (mixed, served_gate, served_up, served_down, held_gate, held_up, held_down)


def solution(mesh):
    return jax.shard_map(
        on_device,
        mesh=mesh,
        in_specs=(
            P(("grp", "fs", "tp"), None),
            P(("grp", "fs", "tp"), None),
            P(("grp", "fs", "tp"), None),
            P("fs"),
            P(None, "fs", "tp"),
            P(None, "fs", "tp"),
            P(None, "fs", "tp"),
            P("fs", "tp"),
            P("fs", "tp"),
            P("fs", "tp"),
        ),
        out_specs=(
            P(("grp", "fs", "tp"), None),
            P(("grp", "fs", "tp"), None, None),
            P(("grp", "fs", "tp"), None, None),
            P(("grp", "fs", "tp"), None, None),
            P(("grp", "fs"), None),
            P(("grp", "fs"), None),
            P(("grp", "fs"), None),
        ),
        check_vma=False,
    )
```

profile of v0, /device:TPU:11, one launch (start us, length us, event | category | flops | bytes accessed | tf_op | source)
XLA Modules:
  0.0 485.5 jit_solution(11063605218181208656)
XLA Ops:
  7.2 3.8 fusion.10
  11.0 31.1 %all_to_all.37 = bf16[16,1,512,64]{2,3,1,0:T(8,128)(2,1)S(1)} all-to-all(bf16[16,1,512,64]{2,3,1,0:T(8,128)(2,1)S(1)} %get-tuple-element.36), channel_id=1, replica_groups=mesh['grp'=2,'fs'=4,'tp'=4] {'fs','tp'}, dimensions={0} | all-to-all | bytes 2097152 | tf_op jit(solution)/shard_map/all_to_all | solution.py:45
  42.1 5.0 %all-to-all-start.2 = ((bf16[16,1,512,64]{2,3,1,0:T(8,128)(2,1)}), bf16[16,1,512,64]{2,3,1,0:T(8,128)(2,1)S(1)}, u32[]{:S(2)}, u32[]{:S(2)}) async-start(bf16[16,1,512,64]{2,3,1,0:T(8,128)(2,1)} %get-tuple-element.37), calls=%async_computation.2 | async-start | bytes 2097152 | tf_op jit(solution)/shard_map/all_to_all | solution.py:46
  47.1 2.7 convert_bitcast_fusion
  49.9 22.1 %all-to-all-done.2 = bf16[16,1,512,64]{2,3,1,0:T(8,128)(2,1)S(1)} async-done(((bf16[16,1,512,64]{2,3,1,0:T(8,128)(2,1)}), bf16[16,1,512,64]{2,3,1,0:T(8,128)(2,1)S(1)}, u32[]{:S(2)}, u32[]{:S(2)}) %all-to-all-start.2) | async-done | bytes 1048608 | tf_op jit(solution)/shard_map/all_to_all | solution.py:46
  72.0 4.8 all-to-all-start.3
  77.1 4.5 reduce-window.6
  82.7 10.2 %scatter_custom_fusion = bf16[1536,2048]{1,0:T(8,128)(2,1)} fusion(s32[1024]{0:T(1024)S(1)} %bitcast.93, bf16[]{:T(256)} %constant.9.clone.1, bf16[128,2048]{1,0:T(8,128)(2,1)S(1)} %fusion.9), kind=kCustom, calls=%fused_computation.5 | custom fusion | bytes 6815746 | tf_op jit(solution)/shard_map/scatter | solution.py:77
  92.9 8.9 %all-to-all-done.3 = bf16[16,1,64,512]{3,2,1,0:T(8,128)(2,1)} async-done(((bf16[16,1,64,512]{3,2,1,0:T(8,128)(2,1)}), bf16[16,1,64,512]{3,2,1,0:T(8,128)(2,1)}, u32[]{:S(2)}, u32[]{:S(2)}) %all-to-all-start.3) | async-done | bytes 1048608 | tf_op jit(solution)/shard_map/all_to_all | solution.py:47
  101.8 4.8 all-to-all-start
  110.8 2.0 copy.77
  114.0 130.0 %all-to-all-done = bf16[16,96,2048]{2,1,0:T(8,128)(2,1)} async-done(((bf16[16,96,2048]{2,1,0:T(8,128)(2,1)}), bf16[16,96,2048]{2,1,0:T(8,128)(2,1)}, u32[]{:S(2)}, u32[]{:S(2)}) %all-to-all-start) | async-done | bytes 6291488 | tf_op jit(solution)/shard_map/all_to_all | solution.py:79
  244.0 6.1 %fusion.25 = f32[1536,256]{1,0:T(8,128)} fusion(bf16[1536,2048]{1,0:T(8,128)(2,1)} %bitcast.6, bf16[2048,256]{0,1:T(8,128)(2,1)} %bitcast.87), kind=kOutput, calls=%fused_computation.51 | convolution fusion | flops 1610612736 | bytes 8912896 | tf_op jit(solution)/shard_map/dot_general | solution.py:11
  250.1 12.9 %convolution_convert_fusion = bf16[1536,2048]{1,0:T(8,128)(2,1)} fusion(bf16[256,2048]{1,0:T(8,128)(2,1)} %bitcast.89, bf16[1536,2048]{1,0:T(8,128)(2,1)} %bitcast.6, bf16[2048,256]{0,1:T(8,128)(2,1)} %bitcast.88, f32[1536,256]{1,0:T(8,128)} %fusion.25), kind=kOutput, calls=%fused_computation.4 | convolution fusion | flops 3226730496 | bytes 16252928 | tf_op jit(solution)/shard_map/dot_general | solution.py:14
  263.0 4.9 %all-to-all-start.4 = ((bf16[16,96,2048]{2,1,0:T(8,128)(2,1)}), bf16[16,96,2048]{2,1,0:T(8,128)(2,1)}, u32[]{:S(2)}, u32[]{:S(2)}) async-start(bf16[16,96,2048]{2,1,0:T(8,128)(2,1)} %bitcast.84), calls=%async_computation.4 | async-start | bytes 12582912 | tf_op jit(solution)/shard_map/all_to_all | solution.py:89
  268.0 29.8 %all_gather.18 = bf16[512,256]{0,1:T(8,128)(2,1)} all-gather(bf16[512,64]{0,1:T(8,128)(2,1)S(1)} %get-tuple-element.34), channel_id=1, replica_groups=mesh['grp'=2,'fs'=4,'tp'=4] {'tp'}, dimensions={1}, use_global_device_ids=true | all-gather | bytes 327680 | tf_op jit(solution)/shard_map/all_gather | solution.py:56
  298.0 10.4 %all_gather.20 = bf16[512,256]{0,1:T(8,128)(2,1)} all-gather(bf16[512,64]{0,1:T(8,128)(2,1)S(1)} %get-tuple-element.35), channel_id=1, replica_groups=mesh['grp'=2,'fs'=4,'tp'=4] {'tp'}, dimensions={1}, use_global_device_ids=true | all-gather | bytes 327680 | tf_op jit(solution)/shard_map/all_gather | solution.py:57
  309.3 8.1 %all_gather.22 = bf16[64,2048]{1,0:T(8,128)(2,1)} all-gather(bf16[64,512]{1,0:T(8,128)(2,1)S(1)} %convert_element_type.63), channel_id=1, replica_groups=mesh['grp'=2,'fs'=4,'tp'=4] {'tp'}, dimensions={1}, use_global_device_ids=true | all-gather | bytes 327680 | tf_op jit(solution)/shard_map/all_gather | solution.py:58
  321.1 52.7 %all-gather.4.cloned.1.call-done = bf16[2048,256]{0,1:T(8,128)(2,1)} async-done(((bf16[512,256]{0,1:T(8,128)(2,1)}), bf16[2048,256]{0,1:T(8,128)(2,1)}) %all-gather.4.cloned.1.call-update) | async-done | bytes 1048592 | tf_op jit(solution)/shard_map/all_gather | solution.py:97
  377.3 2.3 copy.62
  383.2 72.7 %all-to-all-done.4 = bf16[16,96,2048]{2,1,0:T(8,128)(2,1)} async-done(((bf16[16,96,2048]{2,1,0:T(8,128)(2,1)}), bf16[16,96,2048]{2,1,0:T(8,128)(2,1)}, u32[]{:S(2)}, u32[]{:S(2)}) %all-to-all-start.4) | async-done | bytes 6291488 | tf_op jit(solution)/shard_map/all_to_all | solution.py:89
  455.9 12.4 %gather_fusion = bf16[1024,2048]{1,0:T(8,128)(2,1)} fusion(bf16[1536,2048]{1,0:T(8,128)(2,1)} %bitcast.18, s32[1024]{0:T(1024)S(1)} %broadcast_clamp_fusion), kind=kCustom, calls=%fused_computation | custom fusion | bytes 8392704 | tf_op jit(solution)/shard_map/gather | solution.py:90
  468.4 6.5 %fusion = f32[128,2048]{1,0:T(8,128)S(1)} fusion(bf16[1024,2048]{1,0:T(8,128)(2,1)} %gather_fusion, f32[128,8]{1,0:T(8,128)S(1)} %copy.61), kind=kLoop, calls=%fused_computation.3 | loop fusion | flops 6029312 | bytes 5246976 | tf_op jit(solution)/shard_map/reduce_sum | solution.py:91
  475.0 3.3 fusion.5
  (63 shorter events, 19.4 us)
Async XLA Ops:
  42.1 34.7 %copy-start.6 = (s32[128,8]{0,1:T(8,128)S(1)}, s32[128,8]{0,1:T(8,128)}, u32[]{:S(2)}) copy-start(s32[128,8]{0,1:T(8,128)} %param.11) | copy-start | bytes 12292
  42.1 40.2 %copy-start.3 = (bf16[128,2048]{1,0:T(8,128)(2,1)S(1)}, bf16[128,2048]{1,0:T(8,128)(2,1)}, u32[]{:S(2)}) copy-start(bf16[128,2048]{1,0:T(8,128)(2,1)} %param.10) | copy-start | bytes 1572868
  42.1 29.9 %all-to-all-start.2 = ((bf16[16,1,512,64]{2,3,1,0:T(8,128)(2,1)}), bf16[16,1,512,64]{2,3,1,0:T(8,128)(2,1)S(1)}, u32[]{:S(2)}, u32[]{:S(2)}) async-start(bf16[16,1,512,64]{2,3,1,0:T(8,128)(2,1)} %get-tuple-element.37), calls=%async_computation.2 | async-start | bytes 2097152 | tf_op jit(solution)/shard_map/all_to_all | solution.py:46
  72.0 29.8 %all-to-all-start.3 = ((bf16[16,1,64,512]{3,2,1,0:T(8,128)(2,1)}), bf16[16,1,64,512]{3,2,1,0:T(8,128)(2,1)}, u32[]{:S(2)}, u32[]{:S(2)}) async-start(bf16[16,1,64,512]{3,2,1,0:T(8,128)(2,1)} %convert_bitcast_fusion), calls=%async_computation.3 | async-start | bytes 2097152 | tf_op jit(solution)/shard_map/all_to_all | solution.py:47
  82.7 19.1 %copy-start = (bf16[128,2048]{1,0:T(8,128)(2,1)}, bf16[128,2048]{1,0:T(8,128)(2,1)S(1)}, u32[]{:S(2)}) copy-start(bf16[128,2048]{1,0:T(8,128)(2,1)S(1)} %fusion.9) | copy-start | bytes 1572868
  101.8 142.2 %all-to-all-start = ((bf16[16,96,2048]{2,1,0:T(8,128)(2,1)}), bf16[16,96,2048]{2,1,0:T(8,128)(2,1)}, u32[]{:S(2)}, u32[]{:S(2)}) async-start(bf16[16,96,2048]{2,1,0:T(8,128)(2,1)} %bitcast.77), calls=%async_computation | async-start | bytes 12582912 | tf_op jit(solution)/shard_map/all_to_all | solution.py:79
  263.0 5.0 %copy-start.4 = (f32[512,64]{0,1:T(8,128)S(1)}, f32[512,64]{0,1:T(8,128)}, u32[]{:S(2)}) copy-start(f32[512,64]{0,1:T(8,128)} %param.17) | copy-start | bytes 393220
  263.0 5.0 %copy-start.5 = (f32[512,64]{0,1:T(8,128)S(1)}, f32[512,64]{0,1:T(8,128)}, u32[]{:S(2)}) copy-start(f32[512,64]{0,1:T(8,128)} %param.18) | copy-start | bytes 393220
  263.0 5.0 %copy-start.8 = (f32[512]{0:T(512)S(1)}, f32[512]{0:T(512)}, u32[]{:S(2)}) copy-start(f32[512]{0:T(512)} %param.13) | copy-start | bytes 6148
  263.0 58.0 %copy-start.7 = (f32[128,8]{0,1:T(8,128)S(1)}, f32[128,8]{0,1:T(8,128)}, u32[]{:S(2)}) copy-start(f32[128,8]{0,1:T(8,128)} %param.12) | copy-start | bytes 12292
  263.0 192.9 %all-to-all-start.4 = ((bf16[16,96,2048]{2,1,0:T(8,128)(2,1)}), bf16[16,96,2048]{2,1,0:T(8,128)(2,1)}, u32[]{:S(2)}, u32[]{:S(2)}) async-start(bf16[16,96,2048]{2,1,0:T(8,128)(2,1)} %bitcast.84), calls=%async_computation.4 | async-start | bytes 12582912 | tf_op jit(solution)/shard_map/all_to_all | solution.py:89
  267.9 105.9 %all-gather.4.cloned.1.call-start = ((), (), s32[]{:S(2)}) async-start(), calls=%async_computation.5 | async-start | bytes 1310720 | tf_op jit(solution)/shard_map/all_gather | solution.py:97
  297.9 177.0 %all-gather.6.cloned.1.call-start = ((), (), s32[]{:S(2)}) async-start(), calls=%async_computation.6 | async-start | bytes 1310720 | tf_op jit(solution)/shard_map/all_gather | solution.py:102
  308.3 166.6 %all-gather.8.cloned.1.call-start = ((), (), s32[]{:S(2)}) async-start(), calls=%async_computation.7 | async-start | bytes 1310720 | tf_op jit(solution)/shard_map/all_gather | solution.py:109
  468.4 6.6 %copy-start.1 = (bf16[128,2048]{1,0:T(8,128)(2,1)S(1)}, bf16[128,2048]{1,0:T(8,128)(2,1)}, u32[]{:S(2)}) copy-start(bf16[128,2048]{1,0:T(8,128)(2,1)} %copy-done) | copy-start | bytes 1572868
  468.4 9.9 %copy-start.2 = (bf16[64,2048]{1,0:T(8,128)(2,1)S(1)}, bf16[64,2048]{1,0:T(8,128)(2,1)}, u32[]{:S(2)}) copy-start(bf16[64,2048]{1,0:T(8,128)(2,1)} %all_gather.22) | copy-start | bytes 786436
Sparse Core Ops, SparseCore 0:
  298.0 75.7 all-gather.3
  375.4 37.3 all-gather.5
  414.3 35.7 all-gather.7
where the time goes:
time: 486 us; the launch traced here: 485 us
  waiting for transfers between devices  287 us (59%)
  blocking collectives  79.3 us (16%)
  local copies, waits for them, and re-layouts  42.8 us (9%)
  matrix products  24.1 us (5%)
  starting transfers between devices  19.7 us (4%)
  other arithmetic  19.1 us (4%)
  between operations  13.9 us (3%)
    all_to_all x1, waiting for transfers between devices, on_device(): lax.all_to_all(outbox.reshape(experts, capacity, width), ('fs', 'tp'), sp...  130 us
    all_to_all x1, waiting for transfers between devices, on_device(): lax.all_to_all(finished, ('fs', 'tp'), split_axis=0, concat_axis=0, tiled...  72.7 us
    all_gather x1, waiting for transfers between devices, on_device(): lax.all_gather(held_gate, 'fs', axis=0, tiled=True)  52.7 us
    all_to_all x1, blocking collectives, on_device(): lax.all_to_all(piece_gate[:, None], ('fs', 'tp'), split_axis=0, concat_ax...  31.1 us
    all_gather x1, blocking collectives, on_device(): lax.all_gather(tile_gate, 'tp', axis=1, tiled=True)  29.8 us
    all_to_all x1, waiting for transfers between devices, on_device(): lax.all_to_all(piece_up[:, None], ('fs', 'tp'), split_axis=0, concat_axis...  22.1 us
    dot_general x1, matrix products, expert_rows(): jnp.dot(hidden, w_down, preferred_element_type=jnp.float32)  12.9 us
    gather x1, local copies, waits for them, and re-layouts, on_device(): results = returned.reshape(experts * capacity, width)[target]  12.4 us
  transfers between devices with their start and end apart: 7, of which 5 were waited for; matrix products, arithmetic and copies ran while one was open for 12% of the time, Pallas kernels for 0%

commit v1 on v0

--- a/solution.py
+++ b/solution.py
@@ -86,7 +86,20 @@
     finished = expert_rows(
         arrived.reshape(-1, width), served_gate[0], served_up[0], served_down[0]
     ).reshape(arrived.shape)
-    returned = lax.all_to_all(finished, ("fs", "tp"), split_axis=0, concat_axis=0, tiled=True)
+    ready, high = (lax.axis_size(("fs", "tp")), lax.axis_index(("fs", "tp")))
+    oldest = finished.shape[0] // ready
+    outcome_arr = jnp.roll(finished, -high * oldest, axis=0)
+    entries = [lax.slice_in_dim(outcome_arr, 0, oldest, axis=0)]
+    dd = 1
+    while dd < ready:
+        kept_arr = lax.slice_in_dim(outcome_arr, dd * oldest, (dd + 1) * oldest, axis=0)
+        entries.append(
+            lax.ppermute(kept_arr, ("fs", "tp"), [(c, (c + dd) % ready) for c in range(ready)])
+        )
+        dd += 1
+    returned = jnp.roll(
+        jnp.concatenate(entries[::-1], axis=0), (high + 1) * entries[0].shape[0], axis=0
+    )
     results = returned.reshape(experts * capacity, width)[target]
     routed = jnp.sum(
         results.reshape(rows_dev, picks, width).astype(jnp.float32) * weights[:, :, None], axis=1

time: 486 us -> 517 us (1.064); the launches traced: 485 us -> 508 us
  starting transfers between devices: 19.7 us -> 98.6 us
  waiting for transfers between devices: 287 us -> 215 us
  local copies, waits for them, and re-layouts: 42.8 us -> 51.5 us
  other arithmetic: 19.1 us -> 26.9 us
    ppermute x0 -> x15, starting transfers between devices: none -> 83.7 us  [on_device(): lax.ppermute(kept_arr, ('fs', 'tp'), [(c, (c + dd) % ready) for c in rang...]
    all_to_all x1 -> x0, waiting for transfers between devices: 72.7 us -> none  [on_device(): lax.all_to_all(finished, ('fs', 'tp'), split_axis=0, concat_axis=0, tiled...]
    ppermute x0 -> x15, waiting for transfers between devices: none -> 53.6 us  [on_device(): lax.ppermute(kept_arr, ('fs', 'tp'), [(c, (c + dd) % ready) for c in rang...]
    all_gather x1, waiting for transfers between devices: 52.7 us -> 0.01 us  [on_device(): lax.all_gather(held_gate, 'fs', axis=0, tiled=True)]
    concatenate x0 -> x2, other arithmetic: none -> 8.81 us  [the longest x1 4.6 us: on_device(): outcome_arr = jnp.roll(finished, -high * oldest, axis=0)]
    unnamed x27 -> x54, local copies, waits for them, and re-layouts: 11.7 us -> 16.8 us
  transfers between devices with their start and end apart: 7 -> 21, of which waited for: 5 -> 10; matrix products, arithmetic and copies ran while one was open for 12% -> 18% of each run, Pallas kernels for 0% -> 0%
where the time goes in v1:
time: 517 us; the launch traced here: 508 us
  waiting for transfers between devices  215 us (42%)
  starting transfers between devices  98.6 us (19%)
  blocking collectives  77.9 us (15%)
  local copies, waits for them, and re-layouts  51.5 us (10%)
  other arithmetic  26.9 us (5%)
  matrix products  24.1 us (5%)
  between operations  14.2 us (3%)
    all_to_all x1, waiting for transfers between devices, on_device(): lax.all_to_all(outbox.reshape(experts, capacity, width), ('fs', 'tp'), sp...  130 us
    ppermute x15, starting transfers between devices, on_device(): lax.ppermute(kept_arr, ('fs', 'tp'), [(c, (c + dd) % ready) for c in rang...  83.7 us
    ppermute x15, waiting for transfers between devices, on_device(): lax.ppermute(kept_arr, ('fs', 'tp'), [(c, (c + dd) % ready) for c in rang...  53.6 us
    all_to_all x1, blocking collectives, on_device(): lax.all_to_all(piece_gate[:, None], ('fs', 'tp'), split_axis=0, concat_ax...  31.2 us
    all_gather x1, blocking collectives, on_device(): lax.all_gather(tile_gate, 'tp', axis=1, tiled=True)  29.8 us
    all_to_all x1, waiting for transfers between devices, on_device(): lax.all_to_all(piece_up[:, None], ('fs', 'tp'), split_axis=0, concat_axis...  22.1 us
    unnamed x54, local copies, waits for them, and re-layouts  16.8 us
    dot_general x1, matrix products, expert_rows(): jnp.dot(hidden, w_down, preferred_element_type=jnp.float32)  12.9 us
  transfers between devices with their start and end apart: 21, of which 10 were waited for; matrix products, arithmetic and copies ran while one was open for 18% of the time, Pallas kernels for 0%

profile of v1, /device:TPU:11, one launch (start us, length us, event | category | flops | bytes accessed | tf_op | source)
XLA Modules:
  0.0 507.7 jit_solution(11155190601491619431)
XLA Ops:
  11.0 31.2 %all_to_all.32 = bf16[16,1,512,64]{2,3,1,0:T(8,128)(2,1)S(1)} all-to-all(bf16[16,1,512,64]{2,3,1,0:T(8,128)(2,1)S(1)} %get-tuple-element.52), channel_id=1, replica_groups=mesh['grp'=2,'fs'=4,'tp'=4] {'fs','tp'}, dimensions={0} | all-to-all | bytes 2097152 | tf_op jit(solution)/shard_map/all_to_all | solution.py:45
  42.2 4.9 all-to-all-start.2
  49.9 22.1 %all-to-all-done.2 = bf16[16,1,512,64]{2,3,1,0:T(8,128)(2,1)S(1)} async-done(((bf16[16,1,512,64]{2,3,1,0:T(8,128)(2,1)}), bf16[16,1,512,64]{2,3,1,0:T(8,128)(2,1)S(1)}, u32[]{:S(2)}, u32[]{:S(2)}) %all-to-all-start.2) | async-done | bytes 1048608 | tf_op jit(solution)/shard_map/all_to_all | solution.py:46
  72.0 4.8 all-to-all-start.3
  82.7 10.2 %scatter_custom_fusion = bf16[1536,2048]{1,0:T(8,128)(2,1)} fusion(s32[1024]{0:T(1024)S(1)} %bitcast.94, bf16[]{:T(256)} %constant.42.clone.1, bf16[128,2048]{1,0:T(8,128)(2,1)S(1)} %fusion.11), kind=kCustom, calls=%fused_computation.11 | custom fusion | bytes 6815746 | tf_op jit(solution)/shard_map/scatter | solution.py:77
  92.9 8.9 %all-to-all-done.3 = bf16[16,1,64,512]{3,2,1,0:T(8,128)(2,1)} async-done(((bf16[16,1,64,512]{3,2,1,0:T(8,128)(2,1)}), bf16[16,1,64,512]{3,2,1,0:T(8,128)(2,1)}, u32[]{:S(2)}, u32[]{:S(2)}) %all-to-all-start.3) | async-done | bytes 1048608 | tf_op jit(solution)/shard_map/all_to_all | solution.py:47
  101.8 5.0 all-to-all-start
  106.9 29.8 %all_gather.18 = bf16[512,256]{0,1:T(8,128)(2,1)} all-gather(bf16[512,64]{0,1:T(8,128)(2,1)S(1)} %get-tuple-element.50), channel_id=1, replica_groups=mesh['grp'=2,'fs'=4,'tp'=4] {'tp'}, dimensions={1}, use_global_device_ids=true | all-gather | bytes 327680 | tf_op jit(solution)/shard_map/all_gather | solution.py:56
  136.8 10.4 %all_gather.20 = bf16[512,256]{0,1:T(8,128)(2,1)} all-gather(bf16[512,64]{0,1:T(8,128)(2,1)S(1)} %get-tuple-element.51), channel_id=1, replica_groups=mesh['grp'=2,'fs'=4,'tp'=4] {'tp'}, dimensions={1}, use_global_device_ids=true | all-gather | bytes 327680 | tf_op jit(solution)/shard_map/all_gather | solution.py:57
  147.3 6.5 %all_gather.22 = bf16[64,2048]{1,0:T(8,128)(2,1)} all-gather(bf16[64,512]{1,0:T(8,128)(2,1)S(1)} %convert_element_type.63), channel_id=1, replica_groups=mesh['grp'=2,'fs'=4,'tp'=4] {'tp'}, dimensions={1}, use_global_device_ids=true | all-gather | bytes 327680 | tf_op jit(solution)/shard_map/all_gather | solution.py:58
  165.0 129.8 %all-to-all-done = bf16[16,96,2048]{2,1,0:T(8,128)(2,1)} async-done(((bf16[16,96,2048]{2,1,0:T(8,128)(2,1)}), bf16[16,96,2048]{2,1,0:T(8,128)(2,1)}, u32[]{:S(2)}, u32[]{:S(2)}) %all-to-all-start) | async-done | bytes 6291488 | tf_op jit(solution)/shard_map/all_to_all | solution.py:79
  294.8 6.0 %fusion.28 = f32[1536,256]{1,0:T(8,128)} fusion(bf16[1536,2048]{1,0:T(8,128)(2,1)} %bitcast.6, bf16[2048,256]{0,1:T(8,128)(2,1)} %bitcast.88), kind=kOutput, calls=%fused_computation.74 | convolution fusion | flops 1610612736 | bytes 8912896 | tf_op jit(solution)/shard_map/dot_general | solution.py:11
  300.9 12.9 %convolution_convert_fusion = bf16[1536,2048]{1,0:T(8,128)(2,1)} fusion(bf16[256,2048]{1,0:T(8,128)(2,1)} %bitcast.90, bf16[1536,2048]{1,0:T(8,128)(2,1)} %bitcast.6, bf16[2048,256]{0,1:T(8,128)(2,1)} %bitcast.89, f32[1536,256]{1,0:T(8,128)} %fusion.28), kind=kOutput, calls=%fused_computation.8 | convolution fusion | flops 3226730496 | bytes 16252928 | tf_op jit(solution)/shard_map/dot_general | solution.py:14
  313.7 4.6 fusion.2
  348.9 8.8 %collective-permute-start.8 = (bf16[1,96,2048]{2,1,0:T(8,128)(2,1)}, bf16[1,96,2048]{2,1,0:T(8,128)(2,1)S(1)}, u32[]{:S(2)}, u32[]{:S(2)}) collective-permute-start(bf16[1,96,2048]{2,1,0:T(8,128)(2,1)} %get-tuple-element.35), channel_id=1, source_target_pairs={{0,7},{1,8},{2,9},{3,10},{4,11},{5,12},{6,13},{7,14},{8,15},{9,0},... | collective-permute-start | bytes 1179656 | tf_op jit(solution)/shard_map/ppermute | solution.py:97
  357.7 6.3 %collective-permute-done.4 = bf16[1,96,2048]{2,1,0:T(8,128)(2,1)S(1)} collective-permute-done((bf16[1,96,2048]{2,1,0:T(8,128)(2,1)}, bf16[1,96,2048]{2,1,0:T(8,128)(2,1)S(1)}, u32[]{:S(2)}, u32[]{:S(2)}) %collective-permute-start.4) | collective-permute-done | bytes 393248 | tf_op jit(solution)/shard_map/ppermute | solution.py:97
  367.3 6.0 %collective-permute-done.5 = bf16[1,96,2048]{2,1,0:T(8,128)(2,1)S(1)} collective-permute-done((bf16[1,96,2048]{2,1,0:T(8,128)(2,1)}, bf16[1,96,2048]{2,1,0:T(8,128)(2,1)S(1)}, u32[]{:S(2)}, u32[]{:S(2)}) %collective-permute-start.5) | collective-permute-done | bytes 393248 | tf_op jit(solution)/shard_map/ppermute | solution.py:97
  381.7 19.6 %collective-permute-done.7 = bf16[1,96,2048]{2,1,0:T(8,128)(2,1)S(1)} collective-permute-done((bf16[1,96,2048]{2,1,0:T(8,128)(2,1)}, bf16[1,96,2048]{2,1,0:T(8,128)(2,1)S(1)}, u32[]{:S(2)}, u32[]{:S(2)}) %collective-permute-start.7) | collective-permute-done | bytes 393248 | tf_op jit(solution)/shard_map/ppermute | solution.py:97
  401.4 24.1 %collective-permute-start.12 = (bf16[1,96,2048]{2,1,0:T(8,128)(2,1)S(1)}, bf16[1,96,2048]{2,1,0:T(8,128)(2,1)S(1)}, u32[]{:S(2)}, u32[]{:S(2)}) collective-permute-start(bf16[1,96,2048]{2,1,0:T(8,128)(2,1)S(1)} %copy-done.7), channel_id=1, source_target_pairs={{0,3},{1,4},{2,5},{3,6},{4,7},{5,8},{6,9},{7,10},{8,11},{9,12},{10... | collective-permute-start | bytes 1179656 | tf_op jit(solution)/shard_map/ppermute | solution.py:97
  425.6 31.9 %collective-permute-start.13 = (bf16[1,96,2048]{2,1,0:T(8,128)(2,1)S(1)}, bf16[1,96,2048]{2,1,0:T(8,128)(2,1)S(1)}, u32[]{:S(2)}, u32[]{:S(2)}) collective-permute-start(bf16[1,96,2048]{2,1,0:T(8,128)(2,1)S(1)} %copy-done.6), channel_id=1, source_target_pairs={{0,2},{1,3},{2,4},{3,5},{4,6},{5,7},{6,8},{7,9},{8,10},{9,11},{10,... | collective-permute-start | bytes 1179656 | tf_op jit(solution)/shard_map/ppermute | solution.py:97
  457.8 8.6 %collective-permute-done.13 = bf16[1,96,2048]{2,1,0:T(8,128)(2,1)S(1)} collective-permute-done((bf16[1,96,2048]{2,1,0:T(8,128)(2,1)S(1)}, bf16[1,96,2048]{2,1,0:T(8,128)(2,1)S(1)}, u32[]{:S(2)}, u32[]{:S(2)}) %collective-permute-start.13) | collective-permute-done | bytes 393248 | tf_op jit(solution)/shard_map/ppermute | solution.py:97
  466.4 6.5 %collective-permute-done.14 = bf16[1,96,2048]{2,1,0:T(8,128)(2,1)S(1)} collective-permute-done((bf16[1,96,2048]{2,1,0:T(8,128)(2,1)S(1)}, bf16[1,96,2048]{2,1,0:T(8,128)(2,1)S(1)}, u32[]{:S(2)}, u32[]{:S(2)}) %collective-permute-start.14) | collective-permute-done | bytes 393248 | tf_op jit(solution)/shard_map/ppermute | solution.py:97
  478.2 12.5 %gather_fusion = bf16[1024,2048]{1,0:T(8,128)(2,1)} fusion(bf16[1536,2048]{1,0:T(8,128)(2,1)} %bitcast.77, s32[1024]{0:T(1024)S(1)} %broadcast_clamp_fusion), kind=kCustom, calls=%fused_computation | custom fusion | bytes 8392704 | tf_op jit(solution)/shard_map/gather | solution.py:103
  490.6 6.5 %fusion = f32[128,2048]{1,0:T(8,128)S(1)} fusion(bf16[1024,2048]{1,0:T(8,128)(2,1)} %gather_fusion, f32[128,8]{1,0:T(8,128)S(1)} %copy.61), kind=kLoop, calls=%fused_computation.7 | loop fusion | flops 6029312 | bytes 5246976 | tf_op jit(solution)/shard_map/reduce_sum | solution.py:104
  (122 shorter events, 75.6 us)
Async XLA Ops:
  11.0 71.3 %copy-start.4 = (bf16[128,2048]{1,0:T(8,128)(2,1)S(1)}, bf16[128,2048]{1,0:T(8,128)(2,1)}, u32[]{:S(2)}) copy-start(bf16[128,2048]{1,0:T(8,128)(2,1)} %param.12) | copy-start | bytes 1572868
  42.2 29.8 %all-to-all-start.2 = ((bf16[16,1,512,64]{2,3,1,0:T(8,128)(2,1)}), bf16[16,1,512,64]{2,3,1,0:T(8,128)(2,1)S(1)}, u32[]{:S(2)}, u32[]{:S(2)}) async-start(bf16[16,1,512,64]{2,3,1,0:T(8,128)(2,1)} %get-tuple-element.53), calls=%async_computation.2 | async-start | bytes 2097152 | tf_op jit(solution)/shard_map/all_to_all | solution.py:46
  72.0 29.8 %all-to-all-start.3 = ((bf16[16,1,64,512]{3,2,1,0:T(8,128)(2,1)}), bf16[16,1,64,512]{3,2,1,0:T(8,128)(2,1)}, u32[]{:S(2)}, u32[]{:S(2)}) async-start(bf16[16,1,64,512]{3,2,1,0:T(8,128)(2,1)} %convert_bitcast_fusion), calls=%async_computation.3 | async-start | bytes 2097152 | tf_op jit(solution)/shard_map/all_to_all | solution.py:47
  101.8 193.0 %all-to-all-start = ((bf16[16,96,2048]{2,1,0:T(8,128)(2,1)}), bf16[16,96,2048]{2,1,0:T(8,128)(2,1)}, u32[]{:S(2)}, u32[]{:S(2)}) async-start(bf16[16,96,2048]{2,1,0:T(8,128)(2,1)} %bitcast.78), calls=%async_computation | async-start | bytes 12582912 | tf_op jit(solution)/shard_map/all_to_all | solution.py:79
  106.8 216.9 %all-gather.4.cloned.1.call-start = ((), (), s32[]{:S(2)}) async-start(), calls=%async_computation.4 | async-start | bytes 1310720 | tf_op jit(solution)/shard_map/all_gather | solution.py:110
  136.8 360.4 %all-gather.6.cloned.1.call-start = ((), (), s32[]{:S(2)}) async-start(), calls=%async_computation.5 | async-start | bytes 1310720 | tf_op jit(solution)/shard_map/all_gather | solution.py:115
  147.2 350.0 %all-gather.8.cloned.1.call-start = ((), (), s32[]{:S(2)}) async-start(), calls=%async_computation.6 | async-start | bytes 1310720 | tf_op jit(solution)/shard_map/all_gather | solution.py:122
  323.6 14.4 %collective-permute-start = (bf16[1,96,2048]{2,1,0:T(8,128)(2,1)}, bf16[1,96,2048]{2,1,0:T(8,128)(2,1)}, u32[]{:S(2)}, u32[]{:S(2)}) collective-permute-start(bf16[1,96,2048]{2,1,0:T(8,128)(2,1)} %get-tuple-element.43), channel_id=1, source_target_pairs={{0,15},{1,0},{2,1},{3,2},{4,3},{5,4},{6,5},{7,6},{8,7},{9,8},{10,9... | collective-permute-start | bytes 1179656 | tf_op jit(solution)/shard_map/ppermute | solution.py:97
  323.7 16.9 %collective-permute-start.1 = (bf16[1,96,2048]{2,1,0:T(8,128)(2,1)}, bf16[1,96,2048]{2,1,0:T(8,128)(2,1)}, u32[]{:S(2)}, u32[]{:S(2)}) collective-permute-start(bf16[1,96,2048]{2,1,0:T(8,128)(2,1)} %get-tuple-element.42), channel_id=1, source_target_pairs={{0,14},{1,15},{2,0},{3,1},{4,2},{5,3},{6,4},{7,5},{8,6},{9,7},{10,... | collective-permute-start | bytes 1179656 | tf_op jit(solution)/shard_map/ppermute | solution.py:97
  330.2 95.3 %copy-start.6 = (bf16[1,96,2048]{2,1,0:T(8,128)(2,1)S(1)}, bf16[1,96,2048]{2,1,0:T(8,128)(2,1)}, u32[]{:S(2)}) copy-start(bf16[1,96,2048]{2,1,0:T(8,128)(2,1)} %get-tuple-element.30) | copy-start | bytes 1179652
  330.2 127.3 %copy-start.5 = (bf16[1,96,2048]{2,1,0:T(8,128)(2,1)S(1)}, bf16[1,96,2048]{2,1,0:T(8,128)(2,1)}, u32[]{:S(2)}) copy-start(bf16[1,96,2048]{2,1,0:T(8,128)(2,1)} %get-tuple-element.29) | copy-start | bytes 1179652
  333.1 13.3 %collective-permute-start.2 = (bf16[1,96,2048]{2,1,0:T(8,128)(2,1)}, bf16[1,96,2048]{2,1,0:T(8,128)(2,1)S(1)}, u32[]{:S(2)}, u32[]{:S(2)}) collective-permute-start(bf16[1,96,2048]{2,1,0:T(8,128)(2,1)} %get-tuple-element.41), channel_id=1, source_target_pairs={{0,13},{1,14},{2,15},{3,0},{4,1},{5,2},{6,3},{7,4},{8,5},{9,6},{10... | collective-permute-start | bytes 1179656 | tf_op jit(solution)/shard_map/ppermute | solution.py:97
  333.1 15.8 %collective-permute-start.3 = (bf16[1,96,2048]{2,1,0:T(8,128)(2,1)}, bf16[1,96,2048]{2,1,0:T(8,128)(2,1)S(1)}, u32[]{:S(2)}, u32[]{:S(2)}) collective-permute-start(bf16[1,96,2048]{2,1,0:T(8,128)(2,1)} %get-tuple-element.40), channel_id=1, source_target_pairs={{0,12},{1,13},{2,14},{3,15},{4,0},{5,1},{6,2},{7,3},{8,4},{9,5},{1... | collective-permute-start | bytes 1179656 | tf_op jit(solution)/shard_map/ppermute | solution.py:97
  337.0 27.0 %collective-permute-start.4 = (bf16[1,96,2048]{2,1,0:T(8,128)(2,1)}, bf16[1,96,2048]{2,1,0:T(8,128)(2,1)S(1)}, u32[]{:S(2)}, u32[]{:S(2)}) collective-permute-start(bf16[1,96,2048]{2,1,0:T(8,128)(2,1)} %get-tuple-element.39), channel_id=1, source_target_pairs={{0,11},{1,12},{2,13},{3,14},{4,15},{5,0},{6,1},{7,2},{8,3},{9,4},{... | collective-permute-start | bytes 1179656 | tf_op jit(solution)/shard_map/ppermute | solution.py:97
  338.0 35.3 %collective-permute-start.5 = (bf16[1,96,2048]{2,1,0:T(8,128)(2,1)}, bf16[1,96,2048]{2,1,0:T(8,128)(2,1)S(1)}, u32[]{:S(2)}, u32[]{:S(2)}) collective-permute-start(bf16[1,96,2048]{2,1,0:T(8,128)(2,1)} %get-tuple-element.38), channel_id=1, source_target_pairs={{0,10},{1,11},{2,12},{3,13},{4,14},{5,15},{6,0},{7,1},{8,2},{9,3},... | collective-permute-start | bytes 1179656 | tf_op jit(solution)/shard_map/ppermute | solution.py:97
  340.5 39.5 %collective-permute-start.6 = (bf16[1,96,2048]{2,1,0:T(8,128)(2,1)}, bf16[1,96,2048]{2,1,0:T(8,128)(2,1)S(1)}, u32[]{:S(2)}, u32[]{:S(2)}) collective-permute-start(bf16[1,96,2048]{2,1,0:T(8,128)(2,1)} %get-tuple-element.37), channel_id=1, source_target_pairs={{0,9},{1,10},{2,11},{3,12},{4,13},{5,14},{6,15},{7,0},{8,1},{9,2},... | collective-permute-start | bytes 1179656 | tf_op jit(solution)/shard_map/ppermute | solution.py:97
  346.4 55.0 %collective-permute-start.7 = (bf16[1,96,2048]{2,1,0:T(8,128)(2,1)}, bf16[1,96,2048]{2,1,0:T(8,128)(2,1)S(1)}, u32[]{:S(2)}, u32[]{:S(2)}) collective-permute-start(bf16[1,96,2048]{2,1,0:T(8,128)(2,1)} %get-tuple-element.36), channel_id=1, source_target_pairs={{0,8},{1,9},{2,10},{3,11},{4,12},{5,13},{6,14},{7,15},{8,0},{9,1},... | collective-permute-start | bytes 1179656 | tf_op jit(solution)/shard_map/ppermute | solution.py:97
  348.9 76.6 %collective-permute-start.8 = (bf16[1,96,2048]{2,1,0:T(8,128)(2,1)}, bf16[1,96,2048]{2,1,0:T(8,128)(2,1)S(1)}, u32[]{:S(2)}, u32[]{:S(2)}) collective-permute-start(bf16[1,96,2048]{2,1,0:T(8,128)(2,1)} %get-tuple-element.35), channel_id=1, source_target_pairs={{0,7},{1,8},{2,9},{3,10},{4,11},{5,12},{6,13},{7,14},{8,15},{9,0},... | collective-permute-start | bytes 1179656 | tf_op jit(solution)/shard_map/ppermute | solution.py:97
  364.0 93.5 %collective-permute-start.9 = (bf16[1,96,2048]{2,1,0:T(8,128)(2,1)}, bf16[1,96,2048]{2,1,0:T(8,128)(2,1)S(1)}, u32[]{:S(2)}, u32[]{:S(2)}) collective-permute-start(bf16[1,96,2048]{2,1,0:T(8,128)(2,1)} %get-tuple-element.34), channel_id=1, source_target_pairs={{0,6},{1,7},{2,8},{3,9},{4,10},{5,11},{6,12},{7,13},{8,14},{9,15},... | collective-permute-start | bytes 1179656 | tf_op jit(solution)/shard_map/ppermute | solution.py:97
  373.3 84.4 %collective-permute-start.10 = (bf16[1,96,2048]{2,1,0:T(8,128)(2,1)}, bf16[1,96,2048]{2,1,0:T(8,128)(2,1)S(1)}, u32[]{:S(2)}, u32[]{:S(2)}) collective-permute-start(bf16[1,96,2048]{2,1,0:T(8,128)(2,1)} %get-tuple-element.33), channel_id=1, source_target_pairs={{0,5},{1,6},{2,7},{3,8},{4,9},{5,10},{6,11},{7,12},{8,13},{9,14},{... | collective-permute-start | bytes 1179656 | tf_op jit(solution)/shard_map/ppermute | solution.py:97
  380.1 77.6 %collective-permute-start.11 = (bf16[1,96,2048]{2,1,0:T(8,128)(2,1)S(1)}, bf16[1,96,2048]{2,1,0:T(8,128)(2,1)S(1)}, u32[]{:S(2)}, u32[]{:S(2)}) collective-permute-start(bf16[1,96,2048]{2,1,0:T(8,128)(2,1)S(1)} %copy-done.8), channel_id=1, source_target_pairs={{0,4},{1,5},{2,6},{3,7},{4,8},{5,9},{6,10},{7,11},{8,12},{9,13},{1... | collective-permute-start | bytes 1179656 | tf_op jit(solution)/shard_map/ppermute | solution.py:97
  401.4 56.3 %collective-permute-start.12 = (bf16[1,96,2048]{2,1,0:T(8,128)(2,1)S(1)}, bf16[1,96,2048]{2,1,0:T(8,128)(2,1)S(1)}, u32[]{:S(2)}, u32[]{:S(2)}) collective-permute-start(bf16[1,96,2048]{2,1,0:T(8,128)(2,1)S(1)} %copy-done.7), channel_id=1, source_target_pairs={{0,3},{1,4},{2,5},{3,6},{4,7},{5,8},{6,9},{7,10},{8,11},{9,12},{10... | collective-permute-start | bytes 1179656 | tf_op jit(solution)/shard_map/ppermute | solution.py:97
  425.6 40.8 %collective-permute-start.13 = (bf16[1,96,2048]{2,1,0:T(8,128)(2,1)S(1)}, bf16[1,96,2048]{2,1,0:T(8,128)(2,1)S(1)}, u32[]{:S(2)}, u32[]{:S(2)}) collective-permute-start(bf16[1,96,2048]{2,1,0:T(8,128)(2,1)S(1)} %copy-done.6), channel_id=1, source_target_pairs={{0,2},{1,3},{2,4},{3,5},{4,6},{5,7},{6,8},{7,9},{8,10},{9,11},{10,... | collective-permute-start | bytes 1179656 | tf_op jit(solution)/shard_map/ppermute | solution.py:97
  457.5 15.4 %collective-permute-start.14 = (bf16[1,96,2048]{2,1,0:T(8,128)(2,1)S(1)}, bf16[1,96,2048]{2,1,0:T(8,128)(2,1)S(1)}, u32[]{:S(2)}, u32[]{:S(2)}) collective-permute-start(bf16[1,96,2048]{2,1,0:T(8,128)(2,1)S(1)} %copy-done.5), channel_id=1, source_target_pairs={{0,1},{1,2},{2,3},{3,4},{4,5},{5,6},{6,7},{7,8},{8,9},{9,10},{10,1... | collective-permute-start | bytes 1179656 | tf_op jit(solution)/shard_map/ppermute | solution.py:97
  (12 other events, 351.1 us)
Sparse Core Ops, SparseCore 0:
  136.9 75.7 all-gather.3
  214.2 37.3 all-gather.5
  253.2 35.7 all-gather.7
